TPU v7x, 32 devices: a whole 2x2x4 slice. The times are simulated.
32 devices in a mesh: grp: 2 (over x), ep: 4 (over y, core), tp: 4 (over z).
Axes of the slice: x: 2, y: 2, z: 4, core: 2. Of those that a mesh axis runs over, the one named last changes fastest.
Arguments:
- tokens: bfloat16 [2048, 4096], P(('grp', 'ep')), parts along dimension 0, may hold values from -6 to 6
- expert_ids: int32 [2048, 2], P(('grp', 'ep')), parts along dimension 0, may hold values from 0 to 15, as said below
- gates: float32 [2048, 2], P(('grp', 'ep')), parts along dimension 0, may hold values from 0.1 to 1
- w_gate: bfloat16 [16, 4096, 2048], P('ep', None, 'tp'), may hold values from -0.09375 to 0.09375
- w_up: bfloat16 [16, 4096, 2048], P('ep', None, 'tp'), may hold values from -0.09375 to 0.09375
- w_down: bfloat16 [16, 2048, 4096], P('ep', 'tp'), may hold values from -0.79549513 to 0.79549513, as said below
- norm_gain: float32 [4096], P('tp'), may hold values from 0.1 to 1.9
- norm_bias: float32 [4096], P('tp'), may hold values from -1.5 to 1.5
Outputs:
- normed: bfloat16 [2048, 4096], P(('grp', 'ep'), 'tp'), parts along dimension 0
There are 2 independent parts, one for each index of `grp`. A program takes and returns all parts, laid end to end along the dimension named above; an argument that names none is the same for every part. Nothing has to cross between parts.
Inputs may be any that keep to these rules, and one draw needn't show every extreme that they name: `expert_ids`: each row names 2 different experts, both in the same group of 4 consecutive expert numbers. Within one aligned block of 256 rows no expert is named more than 64 times, and in every draw some expert is named exactly 64 times in every block. `w_down`: down projection weights.
All inputs are finite; a program needn't handle non-finite values.
Results may differ from a plain program's by a relative error of at most 0.014.
Values may be sent and summed in bfloat16 or wider, within the bound.
A program may use at most 128 MiB of HBM per device.

v0:
```python
import functools
import jax
import jax.numpy as jnp
from jax import lax
from jax.experimental import pallas as pl
from jax.experimental.pallas import tpu as pltpu
from jax.sharding import PartitionSpec as P

D = 4096
TOPK = 2
EXPERTS = 16
CAP = 64


norm_eps = 1e-05


def route_slots(expert_ids):
    flat_ids = expert_ids.reshape(-1)
    onehot = (flat_ids[:, None] == jnp.arange(EXPERTS, dtype=jnp.int32)[None, :]).astype(jnp.int32)
    position = jnp.sum((jnp.cumsum(onehot, axis=0) - 1) * onehot, axis=1)
    target = flat_ids * CAP + position
    token_of = jnp.arange(flat_ids.shape[0], dtype=jnp.int32) // TOPK
    source = jnp.zeros((EXPERTS * CAP,), jnp.int32).at[target].set(token_of)
    filled = jnp.zeros((EXPERTS * CAP,), jnp.bool_).at[target].set(True)
    return (target, source, filled)


def on_device(tokens, expert_ids, gates, w_gate, w_up, w_down, norm_gain, norm_bias):
    tok_rows, width = tokens.shape
    piece_width = norm_gain.shape[0]
    target, source, filled = route_slots(expert_ids)
    outgoing = jnp.where(filled[:, None], tokens[source], jnp.zeros((), jnp.bfloat16)).reshape(
        EXPERTS, CAP, width
    )
    arrived = lax.all_to_all(outgoing, "ep", split_axis=0, concat_axis=1, tiled=True)
    gate_part = jnp.einsum("erd,edf->erf", arrived, w_gate, preferred_element_type=jnp.float32)
    up_part = jnp.einsum("erd,edf->erf", arrived, w_up, preferred_element_type=jnp.float32)
    hidden = (jax.nn.silu(gate_part) * up_part).astype(jnp.bfloat16)
    partial_value = jnp.einsum("erf,efd->erd", hidden, w_down, preferred_element_type=jnp.float32)
    summed = lax.psum_scatter(
        partial_value.astype(jnp.bfloat16), "tp", scatter_dimension=2, tiled=True
    )
    returned = lax.all_to_all(summed, "ep", split_axis=1, concat_axis=0, tiled=True)
    picked = returned.reshape(EXPERTS * CAP, piece_width)[target].reshape(
        tok_rows, TOPK, piece_width
    )
    combined = jnp.sum(picked.astype(jnp.float32) * gates[:, :, None], axis=1)
    stats = lax.psum((jnp.sum(combined, axis=1), jnp.sum(combined * combined, axis=1)), "tp")
    row_mean = stats[0] / D
    row_var = stats[1] / D - row_mean * row_mean
    normed = (combined - row_mean[:, None]) * lax.rsqrt(
        row_var[:, None] + norm_eps
    ) * norm_gain + norm_bias
    return normed.astype(jnp.bfloat16)


GROUP_EXPERTS = 4
CHUNKS = 16
HALF = CHUNKS // 2
Z_OFFSETS = (2, 2, 1, 1, 3, 3, 0, 0)
PIECES = 8
SENT = 6
LAG = 4
F32 = jnp.float32
BF16 = jnp.bfloat16
MESH = pl.DeviceIdType.MESH


def moe_kernel(
    ids_ref, gates_ref, gain_ref, bias_ref, tokens_ref, wg_ref, wu_ref, wd_ref,
    out_ref,
    tok, wbuf, wd, acc, hid, xr, dnb, place, collect, rowg, meta, meta_in,
    part, core_in, y_in, z_in, st_out, st_in,
    tok_sem, y_send, y_recv, z_send, z_recv, own_send, own_recv, fwd_send, fwd_recv,
    meta_send, meta_recv, w_sem, wd_sem, pc_send, pc_recv, py_send, py_recv,
    pz_send, pz_recv, st_send, st_recv,
):
    ep = lax.axis_index("ep")
    z = lax.axis_index("tp")
    y, c = ep // 2, ep % 2
    partner = y * 2 + (1 - c)
    across = (1 - y) * 2 + c
    diag = (1 - y) * 2 + (1 - c)
    par = z % 2
    zpeer = z + 1 - 2 * par
    rows, width = tokens_ref.shape
    experts = wg_ref.shape[0]
    cols = width // CHUNKS
    piece = gain_ref.shape[1]
    part_cols = piece // 2

    def remote(src, dst, send, recv, e, t):
        return pltpu.make_async_remote_copy(
            src_ref=src, dst_ref=dst, send_sem=send, recv_sem=recv,
            device_id={"ep": e, "tp": t}, device_id_type=MESH,
        )

    def span(ch, size):
        return pl.ds(pl.multiple_of(ch * size, size), size)

    def load_tok(ch):
        return pltpu.make_async_copy(
            tokens_ref.at[:, span(ch, cols)], tok.at[ch, ep], tok_sem.at[ch])

    def load_w(ch, slot):
        return (
            pltpu.make_async_copy(
                wg_ref.at[:, span(ch, cols), :], wbuf.at[slot, 0], w_sem.at[slot, 0]),
            pltpu.make_async_copy(
                wu_ref.at[:, span(ch, cols), :], wbuf.at[slot, 1], w_sem.at[slot, 1]),
        )

    def load_wd(i):
        q = (z + Z_OFFSETS[i]) % 4
        return pltpu.make_async_copy(
            wd_ref.at[:, :, span(q * 2 + i % 2, part_cols)], wd.at[i], wd_sem.at[i])

    def direct(j):
        return par * HALF + j

    def swapped(j):
        return (1 - par) * HALF + j

    def y_copy(j):
        blk = tok.at[direct(j), ep]
        return remote(blk, blk, y_send.at[j], y_recv.at[j], across, z)

    def y_arrive(j):
        blk = tok.at[direct(j), across]
        return remote(blk, blk, y_send.at[j], y_recv.at[j], across, z)

    def z_copy(j):
        blk = tok.at[direct(j), across]
        return remote(blk, blk, z_send.at[j], z_recv.at[j], ep, zpeer)

    def z_arrive(j):
        blk = tok.at[swapped(j), across]
        return remote(blk, blk, z_send.at[j], z_recv.at[j], ep, zpeer)

    def own_copy(ch):
        blk = tok.at[ch, ep]
        return remote(blk, blk, own_send.at[ch], own_recv.at[ch], partner, z)

    def own_arrive(ch):
        blk = tok.at[ch, partner]
        return remote(blk, blk, own_send.at[ch], own_recv.at[ch], partner, z)

    def fwd_copy(ch):
        blk = tok.at[ch, across]
        return remote(blk, blk, fwd_send.at[ch], fwd_recv.at[ch], partner, z)

    def fwd_arrive(ch):
        blk = tok.at[ch, diag]
        return remote(blk, blk, fwd_send.at[ch], fwd_recv.at[ch], partner, z)

    def meta_copy(e, k):
        return remote(meta.at[e], meta_in.at[ep], meta_send.at[k], meta_recv.at[k], e, z)

    def meta_arrive(e, k):
        return remote(meta.at[e], meta_in.at[e], meta_send.at[k], meta_recv.at[k], e, z)

    peers = (partner, across, diag)

    for j in range(HALF):
        load_tok(direct(j)).start()
    for j in range(HALF):
        load_tok(swapped(j)).start()

    barrier = pltpu.get_barrier_semaphore()
    for e in peers:
        pl.semaphore_signal(barrier, inc=1, device_id={"ep": e, "tp": z}, device_id_type=MESH)
    for d in (1, 2, 3):
        pl.semaphore_signal(
            barrier, inc=1, device_id={"ep": ep, "tp": (z + d) % 4}, device_id_type=MESH)
    total_experts = 4 * experts
    expert_row = lax.broadcasted_iota(jnp.int32, (total_experts, rows), 0)
    first = ids_ref[0:1, :] == expert_row
    second = ids_ref[1:2, :] == expert_row
    named = jnp.where(first | second, 1.0, 0.0).astype(F32)
    weight = jnp.where(first, gates_ref[0:1, :], jnp.where(second, gates_ref[1:2, :], 0.0))
    tri_r = lax.broadcasted_iota(jnp.int32, (rows, rows), 0)
    tri_c = lax.broadcasted_iota(jnp.int32, (rows, rows), 1)
    before = jnp.where(tri_r < tri_c, 1.0, 0.0).astype(BF16)
    position = jnp.dot(named.astype(BF16), before, preferred_element_type=F32)
    slot = jnp.where(
        named > 0.5, position + ((expert_row % experts) * CAP).astype(F32), -1.0)
    for e in range(4):
        meta[e, 0:experts, :] = slot[e * experts:(e + 1) * experts, :]
        meta[e, experts:2 * experts, :] = weight[e * experts:(e + 1) * experts, :]
    pl.semaphore_wait(barrier, 6)
    for k, e in enumerate(peers):
        meta_copy(e, k).start()

    for j in range(HALF):
        load_tok(direct(j)).wait()
        y_copy(j).start()
        own_copy(direct(j)).start()
    for j in range(HALF):
        load_tok(swapped(j)).wait()
        own_copy(swapped(j)).start()
    for cp in load_w(direct(0), 0) + load_w(swapped(0), 1):
        cp.start()
    for i in range(PIECES):
        load_wd(i).start()

    meta_in[ep] = meta[ep]
    acc[...] = jnp.zeros_like(acc)
    for k, e in enumerate(peers):
        meta_arrive(e, k).wait_recv()

    row_f = tri_r.astype(F32)
    for s in range(4):
        info = meta_in[s]
        put = jnp.zeros((rows, rows), F32)
        for e in range(experts):
            put += jnp.where(row_f == info[e:e + 1, :], 1.0, 0.0)
        place[s] = put.astype(BF16)
        collect[s] = put.T.astype(BF16)
        for e in range(experts):
            g = jnp.sum(
                put[e * CAP:(e + 1) * CAP, :] * info[experts + e:experts + e + 1, :],
                axis=1, keepdims=True)
            rowg[e, s * CAP:(s + 1) * CAP, :] = jnp.broadcast_to(g, (CAP, 128))

    def work(ch, slot_no):
        for s in range(4):
            x = jnp.dot(place[s], tok[ch, s], preferred_element_type=F32).astype(BF16)
            for e in range(experts):
                xr[e, s * CAP:(s + 1) * CAP, :] = x[e * CAP:(e + 1) * CAP, :]
        for cp in load_w(ch, slot_no):
            cp.wait()

        def one(e, carry):
            for k in range(2):
                acc[k, e] += jnp.dot(xr[e], wbuf[slot_no, k, e], preferred_element_type=F32)
            return carry
        lax.fori_loop(0, experts, one, 0)

    def step(j, carry):
        @pl.when(j < HALF)
        def _():
            y_arrive(j).wait_recv()
            z_copy(j).start()
            fwd_copy(direct(j)).start()

        @pl.when(j >= 1)
        def _():
            z_arrive(j - 1).wait_recv()
            fwd_copy(swapped(j - 1)).start()

        @pl.when(j < HALF)
        def _():
            ch = direct(j)
            own_arrive(ch).wait_recv()
            fwd_arrive(ch).wait_recv()
            work(ch, 0)

            @pl.when(j < HALF - 1)
            def _():
                for cp in load_w(direct(j + 1), 0):
                    cp.start()

        @pl.when(j >= 1)
        def _():
            ch = swapped(j - 1)
            own_arrive(ch).wait_recv()
            fwd_arrive(ch).wait_recv()
            work(ch, 1)

            @pl.when(j < HALF)
            def _():
                for cp in load_w(swapped(j), 1):
                    cp.start()
        return carry
    lax.fori_loop(0, HALF + 1, step, 0)

    def activate(e, carry):
        g = acc[0, e]
        h = g / (1.0 + jnp.exp(-g)) * acc[1, e]
        hid[e] = (h * rowg[e][:, 0:1]).astype(BF16)
        return carry
    lax.fori_loop(0, experts, activate, 0)

    def core_copy(i):
        return remote(part.at[i, 1 - c], core_in.at[i], pc_send.at[i], pc_recv.at[i], partner, z)

    def ret_copy(i):
        return remote(part.at[i, c, 1 - y], y_in.at[i], py_send.at[i], py_recv.at[i], across, z)

    def scatter_copy(i):
        q = (z + Z_OFFSETS[i]) % 4
        return remote(part.at[i, c, y], z_in.at[i], pz_send.at[i], pz_recv.at[i], ep, q)

    for i in range(PIECES + LAG):
        if i < PIECES:
            load_wd(i).wait()

            def down(e, carry):
                o = jnp.dot(hid[e], wd[i, e], preferred_element_type=F32).astype(BF16)
                for s in range(4):
                    dnb[s, span(e, CAP), :] = o[s * CAP:(s + 1) * CAP, :]
                return carry
            lax.fori_loop(0, experts, down, 0)

            def gather(s, carry):
                part[i, s % 2, s // 2] = jnp.dot(
                    collect[s], dnb[s], preferred_element_type=F32).astype(BF16)
                return carry
            lax.fori_loop(0, 4, gather, 0)
            core_copy(i).start()
        if 1 <= i <= PIECES:
            core_copy(i - 1).wait_recv()
            part[i - 1, c, 1 - y] += core_in[i - 1, 1 - y]
            ret_copy(i - 1).start()
        if i >= LAG:
            k = i - LAG
            ret_copy(k).wait_recv()
            part[k, c, y] += core_in[k, y] + y_in[k]
            if k < SENT:
                scatter_copy(k).start()

    halves = []
    for h in range(2):
        half = part[SENT + h, c, y].astype(F32)
        for i in range(h, SENT, 2):
            scatter_copy(i).wait_recv()
            half += z_in[i].astype(F32)
        halves.append(half)
    total = jnp.concatenate(halves, axis=1)

    local_mean = jnp.sum(total, axis=1, keepdims=True) * (1.0 / piece)
    gap = total - local_mean
    local_m2 = jnp.sum(gap * gap, axis=1, keepdims=True)
    mean_t = jnp.broadcast_to(local_mean, (rows, 128)).T
    m2_t = jnp.broadcast_to(local_m2, (rows, 128)).T
    st_out[0:8, :] = mean_t[0:8, :]
    st_out[8:16, :] = m2_t[0:8, :]

    def stat_copy(d):
        return remote(
            st_out, st_in.at[d - 1], st_send.at[d - 1], st_recv.at[d - 1], ep, (z + d) % 4)
    for d in (1, 2, 3):
        stat_copy(d).start()
    for d in (1, 2, 3):
        stat_copy(d).wait_recv()
    means = [st_out[0:8, :]] + [st_in[d, 0:8, :] for d in range(3)]
    m2s = [st_out[8:16, :]] + [st_in[d, 8:16, :] for d in range(3)]
    mean = (means[0] + means[1] + means[2] + means[3]) * 0.25
    m2 = m2s[0] + m2s[1] + m2s[2] + m2s[3]
    for m in means:
        m2 += (m - mean) * (m - mean) * piece
    scale = lax.rsqrt(m2 * (1.0 / width) + norm_eps)
    mean_col = jnp.broadcast_to(mean[0:1, :], (128, rows)).T[:, 0:1]
    scale_col = jnp.broadcast_to(scale[0:1, :], (128, rows)).T[:, 0:1]
    out_ref[...] = (
        (total - mean_col) * scale_col * gain_ref[...] + bias_ref[...]).astype(BF16)

    for j in range(HALF):
        y_copy(j).wait_send()
        z_copy(j).wait_send()
    for ch in range(CHUNKS):
        own_copy(ch).wait_send()
        fwd_copy(ch).wait_send()
    for k, e in enumerate(peers):
        meta_copy(e, k).wait_send()
    for i in range(PIECES):
        core_copy(i).wait_send()
        ret_copy(i).wait_send()
    for i in range(SENT):
        scatter_copy(i).wait_send()
    for d in (1, 2, 3):
        stat_copy(d).wait_send()


def fused_on_device(tokens, expert_ids, gates, w_gate, w_up, w_down, norm_gain, norm_bias):
    rows, width = tokens.shape
    experts, _, hidden = w_gate.shape
    piece = norm_gain.shape[0]
    cols = width // CHUNKS
    part_cols = piece // 2
    dma = pltpu.SemaphoreType.DMA
    vmem = pl.BlockSpec(memory_space=pltpu.VMEM)
    hbm = pl.BlockSpec(memory_space=pl.ANY)
    return pl.pallas_call(
        moe_kernel,
        out_shape=jax.ShapeDtypeStruct((rows, piece), jnp.bfloat16),
        in_specs=[vmem] * 4 + [hbm] * 4,
        out_specs=vmem,
        scratch_shapes=[
            pltpu.VMEM((CHUNKS, 4, rows, cols), BF16),
            pltpu.VMEM((2, 2, experts, cols, hidden), BF16),
            pltpu.VMEM((PIECES, experts, hidden, part_cols), BF16),
            pltpu.VMEM((2, experts, 4 * CAP, hidden), F32),
            pltpu.VMEM((experts, 4 * CAP, hidden), BF16),
            pltpu.VMEM((experts, 4 * CAP, cols), BF16),
            pltpu.VMEM((4, experts * CAP, part_cols), BF16),
            pltpu.VMEM((4, experts * CAP, rows), BF16),
            pltpu.VMEM((4, rows, experts * CAP), BF16),
            pltpu.VMEM((experts, 4 * CAP, 128), F32),
            pltpu.VMEM((4, 2 * experts, rows), F32),
            pltpu.VMEM((4, 2 * experts, rows), F32),
            pltpu.VMEM((PIECES, 2, 2, rows, part_cols), BF16),
            pltpu.VMEM((PIECES, 2, rows, part_cols), BF16),
            pltpu.VMEM((PIECES, rows, part_cols), BF16),
            pltpu.VMEM((SENT, rows, part_cols), BF16),
            pltpu.VMEM((16, rows), F32),
            pltpu.VMEM((3, 16, rows), F32),
            dma((CHUNKS,)), dma((HALF,)), dma((HALF,)), dma((HALF,)), dma((HALF,)),
            dma((CHUNKS,)), dma((CHUNKS,)), dma((CHUNKS,)), dma((CHUNKS,)),
            dma((3,)), dma((3,)), dma((2, 2)), dma((PIECES,)),
            dma((PIECES,)), dma((PIECES,)), dma((PIECES,)), dma((PIECES,)),
            dma((SENT,)), dma((SENT,)), dma((3,)), dma((3,)),
        ],
        compiler_params=pltpu.CompilerParams(
            collective_id=0, has_side_effects=True, vmem_limit_bytes=64 * 1024 * 1024 - 65536),
    )(
        expert_ids.T, gates.T, norm_gain[None, :], norm_bias[None, :],
        tokens, w_gate, w_up, w_down,
    )


def solution(mesh):
    groups_apart = EXPERTS == GROUP_EXPERTS * mesh.shape["ep"]
    fused = groups_apart and mesh.shape["ep"] == 4 and mesh.shape["tp"] == 4
    return jax.shard_map(
        fused_on_device if fused else on_device,
        mesh=mesh,
        in_specs=(
            P(("grp", "ep"), None),
            P(("grp", "ep"), None),
            P(("grp", "ep"), None),
            P("ep", None, "tp"),
            P("ep", None, "tp"),
            P("ep", "tp", None),
            P("tp"),
            P("tp"),
        ),
        out_specs=P(("grp", "ep"), "tp"),
        check_vma=False,
    )
```

profile of v0, /device:TPU:0, one launch (start us, length us, event | category | flops | bytes accessed | tf_op | source)
XLA Modules:
  0.0 114.7 jit_solution(10770879230539799901)
XLA Ops:
  0.0 112.8 %shard_map.82 = bf16[256,1024]{1,0:T(8,128)(2,1)} custom-call(s32[2,256]{1,0:T(2,128)} %bitcast.6, f32[2,256]{1,0:T(2,128)} %bitcast.7, f32[1,1024]{1,0:T(1,128)} %bitcast.4, f32[1,1024]{1,0:T(1,128)} %bitcast.5, bf16[256,4096]{1,0:T(8,128)(2,1)} %tokens_ref.1, bf16[4,4096,512]{2,1,0:T(8,128)(2,1)} %wg_ref.1, bf16[4,4096,512]{2,1,0:T(8,128)(2,1)} %wu_ref.1, ...), custom_call_target="tpu_custom_call" | custom-call | tf_op jit(solution)/shard_map/pallas_call | solution.py:385
  112.8 1.9 %copy.10 = bf16[256,1024]{1,0:T(8,128)(2,1)} copy(bf16[256,1024]{1,0:T(8,128)(2,1)} %shard_map.82) | data formatting | bytes 1048576
where the time goes:
time: 115 us
  Pallas kernels  113 us (98%)
  local copies, waits for them, and re-layouts  1.87 us (2%)
    pallas_call x1, Pallas kernels, fused_on_device(): pl.pallas_call(moe_kernel, out_shape=jax.ShapeDtypeStruct((rows, piece),...  113 us

commit v1 on v0

v1 whole, which is shorter than its diff:
```python
import functools
import jax
import jax.numpy as jnp
from jax import lax
from jax.experimental import pallas as pl
from jax.experimental.pallas import tpu as pltpu
from jax.sharding import PartitionSpec as P

D = 4096
TOPK = 2
EXPERTS = 16
CAP = 64


norm_eps = 1e-05


def route_slots(expert_ids):
    flat_ids = expert_ids.reshape(-1)
    onehot = (flat_ids[:, None] == jnp.arange(EXPERTS, dtype=jnp.int32)[None, :]).astype(jnp.int32)
    position = jnp.sum((jnp.cumsum(onehot, axis=0) - 1) * onehot, axis=1)
    target = flat_ids * CAP + position
    token_of = jnp.arange(flat_ids.shape[0], dtype=jnp.int32) // TOPK
    source = jnp.zeros((EXPERTS * CAP,), jnp.int32).at[target].set(token_of)
    filled = jnp.zeros((EXPERTS * CAP,), jnp.bool_).at[target].set(True)
    return (target, source, filled)


def on_device(tokens, expert_ids, gates, w_gate, w_up, w_down, norm_gain, norm_bias):
    tok_rows, width = tokens.shape
    piece_width = norm_gain.shape[0]
    target, source, filled = route_slots(expert_ids)
    outgoing = jnp.where(filled[:, None], tokens[source], jnp.zeros((), jnp.bfloat16)).reshape(
        EXPERTS, CAP, width
    )
    arrived = lax.all_to_all(outgoing, "ep", split_axis=0, concat_axis=1, tiled=True)
    gate_part = jnp.einsum("erd,edf->erf", arrived, w_gate, preferred_element_type=jnp.float32)
    up_part = jnp.einsum("erd,edf->erf", arrived, w_up, preferred_element_type=jnp.float32)
    hidden = (jax.nn.silu(gate_part) * up_part).astype(jnp.bfloat16)
    partial_value = jnp.einsum("erf,efd->erd", hidden, w_down, preferred_element_type=jnp.float32)
    summed = lax.psum_scatter(
        partial_value.astype(jnp.bfloat16), "tp", scatter_dimension=2, tiled=True
    )
    returned = lax.all_to_all(summed, "ep", split_axis=1, concat_axis=0, tiled=True)
    picked = returned.reshape(EXPERTS * CAP, piece_width)[target].reshape(
        tok_rows, TOPK, piece_width
    )
    combined = jnp.sum(picked.astype(jnp.float32) * gates[:, :, None], axis=1)
    stats = lax.psum((jnp.sum(combined, axis=1), jnp.sum(combined * combined, axis=1)), "tp")
    row_mean = stats[0] / D
    row_var = stats[1] / D - row_mean * row_mean
    normed = (combined - row_mean[:, None]) * lax.rsqrt(
        row_var[:, None] + norm_eps
    ) * norm_gain + norm_bias
    return normed.astype(jnp.bfloat16)


GROUP_EXPERTS = 4
CHUNKS = 16
HALF = CHUNKS // 2
PASSES = 2
SLOTS = 3
PIECES = 8
SENT = 6
EARLY = 6
F32 = jnp.float32
BF16 = jnp.bfloat16
MESH = pl.DeviceIdType.MESH


def moe_kernel(
    ids_ref, gates_ref, gain_ref, bias_ref, tokens_ref, wg_ref, wu_ref, wd_ref,
    out_ref,
    tok, wbuf, wd, acc, hid, xr, dnb, place, collect, rowg, meta, meta_in,
    part, core_in, y_in, z_in, st_out, st_in,
    tok_sem, y_send, y_recv, z_send, z_recv, own_send, own_recv, fwd_send, fwd_recv,
    meta_send, meta_recv, w_sem, wd_sem, pc_send, pc_recv, py_send, py_recv,
    pz_send, pz_recv, st_send, st_recv,
):
    ep = lax.axis_index("ep")
    z = lax.axis_index("tp")
    y, c = ep // 2, ep % 2
    partner = y * 2 + (1 - c)
    across = (1 - y) * 2 + c
    diag = (1 - y) * 2 + (1 - c)
    par = z % 2
    zpeer = z + 1 - 2 * par
    rows, width = tokens_ref.shape
    band = rows // PASSES
    experts = wg_ref.shape[0]
    cols = width // CHUNKS
    piece = gain_ref.shape[1]
    part_cols = piece // 2

    def remote(src, dst, send, recv, e, t):
        return pltpu.make_async_remote_copy(
            src_ref=src, dst_ref=dst, send_sem=send, recv_sem=recv,
            device_id={"ep": e, "tp": t}, device_id_type=MESH,
        )

    def span(ch, size):
        return pl.ds(pl.multiple_of(ch * size, size), size)

    def load_tok(ch):
        return pltpu.make_async_copy(
            tokens_ref.at[:, span(ch, cols)], tok.at[ch, ep], tok_sem.at[ch])

    def band_rows(h):
        return pl.ds(h * band, band)

    def zshift(i):
        return (z + 3 - i // 2) % 4

    def load_wd(i):
        return pltpu.make_async_copy(
            wd_ref.at[:, :, span(zshift(i) * 2 + i % 2, part_cols)], wd.at[i], wd_sem.at[i])

    def direct(j):
        return par * HALF + j

    def swapped(j):
        return (1 - par) * HALF + j

    def load_unit(t):
        u, slot = t % HALF, t % SLOTS
        return [
            pltpu.make_async_copy(
                w_ref.at[:, span(ch, cols), :],
                wbuf.at[slot, g, :, pl.ds(k * cols, cols), :], w_sem.at[slot, g, k])
            for k, ch in enumerate((direct(u), swapped(u)))
            for g, w_ref in enumerate((wg_ref, wu_ref))
        ]

    def y_copy(h, j):
        blk = tok.at[direct(j), ep, band_rows(h)]
        return remote(blk, blk, y_send.at[h, j], y_recv.at[h, j], across, z)

    def y_arrive(h, j):
        blk = tok.at[direct(j), across, band_rows(h)]
        return remote(blk, blk, y_send.at[h, j], y_recv.at[h, j], across, z)

    def z_copy(h, j):
        blk = tok.at[direct(j), across, band_rows(h)]
        return remote(blk, blk, z_send.at[h, j], z_recv.at[h, j], ep, zpeer)

    def z_arrive(h, j):
        blk = tok.at[swapped(j), across, band_rows(h)]
        return remote(blk, blk, z_send.at[h, j], z_recv.at[h, j], ep, zpeer)

    def own_copy(h, ch):
        blk = tok.at[ch, ep, band_rows(h)]
        return remote(blk, blk, own_send.at[h, ch], own_recv.at[h, ch], partner, z)

    def own_arrive(h, ch):
        blk = tok.at[ch, partner, band_rows(h)]
        return remote(blk, blk, own_send.at[h, ch], own_recv.at[h, ch], partner, z)

    def fwd_copy(h, ch):
        blk = tok.at[ch, across, band_rows(h)]
        return remote(blk, blk, fwd_send.at[h, ch], fwd_recv.at[h, ch], partner, z)

    def fwd_arrive(h, ch):
        blk = tok.at[ch, diag, band_rows(h)]
        return remote(blk, blk, fwd_send.at[h, ch], fwd_recv.at[h, ch], partner, z)

    def meta_copy(e, k):
        return remote(meta.at[e], meta_in.at[ep], meta_send.at[k], meta_recv.at[k], e, z)

    def meta_arrive(e, k):
        return remote(meta.at[e], meta_in.at[e], meta_send.at[k], meta_recv.at[k], e, z)

    peers = (partner, across, diag)

    for j in range(HALF):
        load_tok(direct(j)).start()
    for j in range(HALF):
        load_tok(swapped(j)).start()
    for t in range(SLOTS):
        for cp in load_unit(t):
            cp.start()

    barrier = pltpu.get_barrier_semaphore()
    for e in peers:
        pl.semaphore_signal(barrier, inc=1, device_id={"ep": e, "tp": z}, device_id_type=MESH)
    for d in (1, 2, 3):
        pl.semaphore_signal(
            barrier, inc=1, device_id={"ep": ep, "tp": (z + d) % 4}, device_id_type=MESH)
    total_experts = 4 * experts
    expert_row = lax.broadcasted_iota(jnp.int32, (total_experts, rows), 0)
    first = ids_ref[0:1, :] == expert_row
    second = ids_ref[1:2, :] == expert_row
    named = jnp.where(first | second, 1.0, 0.0).astype(F32)
    weight = jnp.where(first, gates_ref[0:1, :], jnp.where(second, gates_ref[1:2, :], 0.0))
    tri_r = lax.broadcasted_iota(jnp.int32, (rows, rows), 0)
    tri_c = lax.broadcasted_iota(jnp.int32, (rows, rows), 1)
    before = jnp.where(
        (tri_r < tri_c) & (tri_r // band == tri_c // band), 1.0, 0.0).astype(BF16)
    position = jnp.dot(named.astype(BF16), before, preferred_element_type=F32)
    slot = jnp.where(
        named > 0.5, position + ((expert_row % experts) * CAP).astype(F32), -1.0)
    for e in range(4):
        meta[e, 0:experts, :] = slot[e * experts:(e + 1) * experts, :]
        meta[e, experts:2 * experts, :] = weight[e * experts:(e + 1) * experts, :]
    pl.semaphore_wait(barrier, 6)
    for k, e in enumerate(peers):
        meta_copy(e, k).start()

    for j in range(HALF):
        load_tok(direct(j)).wait()
        y_copy(0, j).start()
        own_copy(0, direct(j)).start()
    for j in range(HALF):
        load_tok(swapped(j)).wait()
        own_copy(0, swapped(j)).start()
    for j in range(HALF):
        y_copy(1, j).start()
    for ch in range(CHUNKS):
        own_copy(1, ch).start()
    for i in range(PIECES):
        load_wd(i).start()

    meta_in[ep] = meta[ep]
    acc[...] = jnp.zeros_like(acc)
    for k, e in enumerate(peers):
        meta_arrive(e, k).wait_recv()

    row_f = tri_r.astype(F32)
    for s in range(4):
        info = meta_in[s]
        put = jnp.zeros((rows, rows), F32)
        for e in range(experts):
            put += jnp.where(row_f == info[e:e + 1, :], 1.0, 0.0)
        back = put.T
        for h in range(PASSES):
            mine = slice(h * band, (h + 1) * band)
            place[h, s] = put[:, mine].astype(BF16)
            collect[h, s] = back[mine, :].astype(BF16)
            for e in range(experts):
                g = jnp.sum(
                    put[e * CAP:(e + 1) * CAP, mine]
                    * info[experts + e:experts + e + 1, mine],
                    axis=1, keepdims=True)
                rowg[h, e, s * CAP:(s + 1) * CAP, :] = jnp.broadcast_to(g, (CAP, 128))

    def unit(h, u):
        t = h * HALF + u
        for k, ch in enumerate((direct(u), swapped(u))):
            own_arrive(h, ch).wait_recv()
            fwd_arrive(h, ch).wait_recv()
            for s in range(4):
                x = jnp.dot(
                    place[h, s], tok[ch, s, band_rows(h), :],
                    preferred_element_type=F32).astype(BF16)
                for e in range(experts):
                    xr[e, s * CAP:(s + 1) * CAP, k * cols:(k + 1) * cols] = (
                        x[e * CAP:(e + 1) * CAP, :])
        for cp in load_unit(t):
            cp.wait()

        def one(e, carry):
            for g in range(2):
                acc[g, e] += jnp.dot(xr[e], wbuf[t % SLOTS, g, e], preferred_element_type=F32)
            return carry
        lax.fori_loop(0, experts, one, 0)

        @pl.when(t + SLOTS < PASSES * HALF)
        def _():
            for cp in load_unit(t + SLOTS):
                cp.start()

    def relay(h, j):
        @pl.when(j < HALF)
        def _():
            y_arrive(h, j).wait_recv()
            z_copy(h, j).start()
            fwd_copy(h, direct(j)).start()

        @pl.when((j >= 1) & (j <= HALF))
        def _():
            z_arrive(h, j - 1).wait_recv()
            fwd_copy(h, swapped(j - 1)).start()

    def activate(h):
        def one(e, carry):
            g = acc[0, e]
            v = g / (1.0 + jnp.exp(-g)) * acc[1, e]
            hid[e] = (v * rowg[h, e][:, 0:1]).astype(BF16)
            if h + 1 < PASSES:
                acc[0, e] = jnp.zeros_like(g)
                acc[1, e] = jnp.zeros_like(g)
            return carry
        lax.fori_loop(0, experts, one, 0)

    def core_copy(h, i):
        return remote(
            part.at[i, 1 - c, :, band_rows(h)], core_in.at[i, :, band_rows(h)],
            pc_send.at[h, i], pc_recv.at[h, i], partner, z)

    def ret_copy(h, i):
        return remote(
            part.at[i, c, 1 - y, band_rows(h)], y_in.at[i, band_rows(h)],
            py_send.at[h, i], py_recv.at[h, i], across, z)

    def scatter_copy(h, i):
        return remote(
            part.at[i, c, y, band_rows(h)], z_in.at[i, band_rows(h)],
            pz_send.at[h, i], pz_recv.at[h, i], ep, zshift(i))

    def down(h, i):
        if h == 0:
            load_wd(i).wait()

        def one(e, carry):
            o = jnp.dot(hid[e], wd[i, e], preferred_element_type=F32).astype(BF16)
            for s in range(4):
                dnb[s, span(e, CAP), :] = o[s * CAP:(s + 1) * CAP, :]
            return carry
        lax.fori_loop(0, experts, one, 0)

        def gather(s, carry):
            part[i, s % 2, s // 2, band_rows(h), :] = jnp.dot(
                collect[h, s], dnb[s], preferred_element_type=F32).astype(BF16)
            return carry
        lax.fori_loop(0, 4, gather, 0)
        core_copy(h, i).start()

    def give_back(h, i):
        core_copy(h, i).wait_recv()
        part[i, c, 1 - y, band_rows(h), :] += core_in[i, 1 - y, band_rows(h), :]
        ret_copy(h, i).start()

    def settle(h, k):
        ret_copy(h, k).wait_recv()
        part[k, c, y, band_rows(h), :] += (
            core_in[k, y, band_rows(h), :] + y_in[k, band_rows(h), :])

        @pl.when(k < SENT)
        def _():
            scatter_copy(h, k).start()

    def first_pass(j, carry):
        relay(0, j)

        @pl.when(j >= 2)
        def _():
            unit(0, j - 2)
        return carry
    lax.fori_loop(0, HALF + 2, first_pass, 0)
    activate(0)

    def second_pass(j, carry):
        relay(1, j)

        @pl.when((j >= 1) & (j <= PIECES))
        def _():
            give_back(0, j - 1)

        @pl.when(j < PIECES)
        def _():
            down(0, j)

        @pl.when(j >= 2)
        def _():
            unit(1, j - 2)

        @pl.when(j >= EARLY)
        def _():
            settle(0, j - EARLY)
        return carry
    lax.fori_loop(0, HALF + 2, second_pass, 0)
    activate(1)
    settled = HALF + 2 - EARLY

    def last_down(i, carry):
        @pl.when(i < PIECES)
        def _():
            down(1, i)

        @pl.when(i >= 1)
        def _():
            give_back(1, i - 1)

        @pl.when(i < PIECES - settled)
        def _():
            settle(0, i + settled)
        return carry
    lax.fori_loop(0, PIECES + 1, last_down, 0)

    def last_settle(k, carry):
        settle(1, k)
        return carry
    lax.fori_loop(0, PIECES, last_settle, 0)

    halves = []
    for n in range(2):
        half = part[SENT + n, c, y].astype(F32)
        for i in range(n, SENT, 2):
            for h in range(PASSES):
                scatter_copy(h, i).wait_recv()
            half += z_in[i].astype(F32)
        halves.append(half)
    total = jnp.concatenate(halves, axis=1)

    local_mean = jnp.sum(total, axis=1, keepdims=True) * (1.0 / piece)
    gap = total - local_mean
    local_m2 = jnp.sum(gap * gap, axis=1, keepdims=True)
    mean_t = jnp.broadcast_to(local_mean, (rows, 128)).T
    m2_t = jnp.broadcast_to(local_m2, (rows, 128)).T
    st_out[0:8, :] = mean_t[0:8, :]
    st_out[8:16, :] = m2_t[0:8, :]

    def stat_copy(d):
        return remote(
            st_out, st_in.at[d - 1], st_send.at[d - 1], st_recv.at[d - 1], ep, (z + d) % 4)
    for d in (1, 2, 3):
        stat_copy(d).start()
    for d in (1, 2, 3):
        stat_copy(d).wait_recv()
    means = [st_out[0:8, :]] + [st_in[d, 0:8, :] for d in range(3)]
    m2s = [st_out[8:16, :]] + [st_in[d, 8:16, :] for d in range(3)]
    mean = (means[0] + means[1] + means[2] + means[3]) * 0.25
    m2 = m2s[0] + m2s[1] + m2s[2] + m2s[3]
    for m in means:
        m2 += (m - mean) * (m - mean) * piece
    scale = lax.rsqrt(m2 * (1.0 / width) + norm_eps)
    mean_col = jnp.broadcast_to(mean[0:1, :], (128, rows)).T[:, 0:1]
    scale_col = jnp.broadcast_to(scale[0:1, :], (128, rows)).T[:, 0:1]
    out_ref[...] = (
        (total - mean_col) * scale_col * gain_ref[...] + bias_ref[...]).astype(BF16)

    def sent_tokens(j, carry):
        for h in range(PASSES):
            y_copy(h, j).wait_send()
            z_copy(h, j).wait_send()
            for ch in (direct(j), swapped(j)):
                own_copy(h, ch).wait_send()
                fwd_copy(h, ch).wait_send()
        return carry
    lax.fori_loop(0, HALF, sent_tokens, 0)
    for k, e in enumerate(peers):
        meta_copy(e, k).wait_send()
    for h in range(PASSES):
        for i in range(PIECES):
            core_copy(h, i).wait_send()
            ret_copy(h, i).wait_send()
        for i in range(SENT):
            scatter_copy(h, i).wait_send()
    for d in (1, 2, 3):
        stat_copy(d).wait_send()


def fused_on_device(tokens, expert_ids, gates, w_gate, w_up, w_down, norm_gain, norm_bias):
    rows, width = tokens.shape
    experts, _, hidden = w_gate.shape
    piece = norm_gain.shape[0]
    cols = width // CHUNKS
    part_cols = piece // 2
    band = rows // PASSES
    dma = pltpu.SemaphoreType.DMA
    vmem = pl.BlockSpec(memory_space=pltpu.VMEM)
    hbm = pl.BlockSpec(memory_space=pl.ANY)
    return pl.pallas_call(
        moe_kernel,
        out_shape=jax.ShapeDtypeStruct((rows, piece), jnp.bfloat16),
        in_specs=[vmem] * 4 + [hbm] * 4,
        out_specs=vmem,
        scratch_shapes=[
            pltpu.VMEM((CHUNKS, 4, rows, cols), BF16),
            pltpu.VMEM((SLOTS, 2, experts, 2 * cols, hidden), BF16),
            pltpu.VMEM((PIECES, experts, hidden, part_cols), BF16),
            pltpu.VMEM((2, experts, 4 * CAP, hidden), F32),
            pltpu.VMEM((experts, 4 * CAP, hidden), BF16),
            pltpu.VMEM((experts, 4 * CAP, 2 * cols), BF16),
            pltpu.VMEM((4, experts * CAP, part_cols), BF16),
            pltpu.VMEM((PASSES, 4, experts * CAP, band), BF16),
            pltpu.VMEM((PASSES, 4, band, experts * CAP), BF16),
            pltpu.VMEM((PASSES, experts, 4 * CAP, 128), F32),
            pltpu.VMEM((4, 2 * experts, rows), F32),
            pltpu.VMEM((4, 2 * experts, rows), F32),
            pltpu.VMEM((PIECES, 2, 2, rows, part_cols), BF16),
            pltpu.VMEM((PIECES, 2, rows, part_cols), BF16),
            pltpu.VMEM((PIECES, rows, part_cols), BF16),
            pltpu.VMEM((SENT, rows, part_cols), BF16),
            pltpu.VMEM((16, rows), F32),
            pltpu.VMEM((3, 16, rows), F32),
            dma((CHUNKS,)), dma((PASSES, HALF)), dma((PASSES, HALF)),
            dma((PASSES, HALF)), dma((PASSES, HALF)),
            dma((PASSES, CHUNKS)), dma((PASSES, CHUNKS)),
            dma((PASSES, CHUNKS)), dma((PASSES, CHUNKS)),
            dma((3,)), dma((3,)), dma((SLOTS, 2, 2)), dma((PIECES,)),
            dma((PASSES, PIECES)), dma((PASSES, PIECES)),
            dma((PASSES, PIECES)), dma((PASSES, PIECES)),
            dma((PASSES, SENT)), dma((PASSES, SENT)), dma((3,)), dma((3,)),
        ],
        compiler_params=pltpu.CompilerParams(
            collective_id=0, has_side_effects=True, vmem_limit_bytes=64 * 1024 * 1024 - 65536),
    )(
        expert_ids.T, gates.T, norm_gain[None, :], norm_bias[None, :],
        tokens, w_gate, w_up, w_down,
    )


def solution(mesh):
    groups_apart = EXPERTS == GROUP_EXPERTS * mesh.shape["ep"]
    fused = groups_apart and mesh.shape["ep"] == 4 and mesh.shape["tp"] == 4
    return jax.shard_map(
        fused_on_device if fused else on_device,
        mesh=mesh,
        in_specs=(
            P(("grp", "ep"), None),
            P(("grp", "ep"), None),
            P(("grp", "ep"), None),
            P("ep", None, "tp"),
            P("ep", None, "tp"),
            P("ep", "tp", None),
            P("tp"),
            P("tp"),
        ),
        out_specs=P(("grp", "ep"), "tp"),
        check_vma=False,
    )
```

time: 115 us -> 131 us (1.14)
  Pallas kernels: 113 us -> 129 us
    pallas_call x1, Pallas kernels: 113 us -> 129 us  [fused_on_device(): pl.pallas_call(moe_kernel, out_shape=jax.ShapeDtypeStruct((rows, piece),...]
where the time goes in v1:
time: 131 us; the launch traced here: 130 us
  Pallas kernels  129 us (98%)
  local copies, waits for them, and re-layouts  1.87 us (1%)
    pallas_call x1, Pallas kernels, fused_on_device(): pl.pallas_call(moe_kernel, out_shape=jax.ShapeDtypeStruct((rows, piece),...  129 us

profile of v1, /device:TPU:0, one launch (start us, length us, event | category | flops | bytes accessed | tf_op | source)
XLA Modules:
  0.0 130.4 jit_solution(2120123093623019582)
XLA Ops:
  0.0 128.5 %shard_map.82 = bf16[256,1024]{1,0:T(8,128)(2,1)} custom-call(s32[2,256]{1,0:T(2,128)} %bitcast.6, f32[2,256]{1,0:T(2,128)} %bitcast.7, f32[1,1024]{1,0:T(1,128)} %bitcast.4, f32[1,1024]{1,0:T(1,128)} %bitcast.5, bf16[256,4096]{1,0:T(8,128)(2,1)} %tokens_ref.1, bf16[4,4096,512]{2,1,0:T(8,128)(2,1)} %wg_ref.1, bf16[4,4096,512]{2,1,0:T(8,128)(2,1)} %wu_ref.1, ...), custom_call_target="tpu_custom_call" | custom-call | tf_op jit(solution)/shard_map/pallas_call | solution.py:462
  128.5 1.9 %copy.10 = bf16[256,1024]{1,0:T(8,128)(2,1)} copy(bf16[256,1024]{1,0:T(8,128)(2,1)} %shard_map.82) | data formatting | bytes 1048576

commit v2 on v1

--- a/solution.py
+++ b/solution.py
@@ -62,7 +62,8 @@
 SLOTS = 3
 PIECES = 8
 SENT = 6
-EARLY = 6
+HOP = 2
+EARLY = 2
 F32 = jnp.float32
 BF16 = jnp.bfloat16
 MESH = pl.DeviceIdType.MESH
@@ -83,7 +84,7 @@
     partner = y * 2 + (1 - c)
     across = (1 - y) * 2 + c
     diag = (1 - y) * 2 + (1 - c)
-    par = z % 2
+    par, side = z % 2, z // 2
     zpeer = z + 1 - 2 * par
     rows, width = tokens_ref.shape
     band = rows // PASSES
@@ -106,14 +107,20 @@
             tokens_ref.at[:, span(ch, cols)], tok.at[ch, ep], tok_sem.at[ch])
 
     def band_rows(h):
-        return pl.ds(h * band, band)
-
-    def zshift(i):
-        return (z + 3 - i // 2) % 4
+        return pl.ds(pl.multiple_of(h * band, band), band)
+
+    def flip(far, near):
+        return 2 * (side + far - 2 * side * far) + par + near - 2 * par * near
+
+    def target(i):
+        return flip((3 - i // 2) // 2, (3 - i // 2) % 2)
+
+    def next_hop(i):
+        return flip((i // 2) % 2, 1 - (i // 2) % 2)
 
     def load_wd(i):
         return pltpu.make_async_copy(
-            wd_ref.at[:, :, span(zshift(i) * 2 + i % 2, part_cols)], wd.at[i], wd_sem.at[i])
+            wd_ref.at[:, :, span(target(i) * 2 + i % 2, part_cols)], wd.at[i], wd_sem.at[i])
 
     def direct(j):
         return par * HALF + j
@@ -121,13 +128,18 @@
     def swapped(j):
         return (1 - par) * HALF + j
 
+    def unit_chunk(u):
+        late, begun = u // 7, (u + 7) // 8
+        kind = (1 - u % 2) * begun + late
+        index = (u + 1) // 2 - (1 - u % 2) * begun - late
+        return (par + kind - 2 * par * kind) * HALF + 2 * index
+
     def load_unit(t):
-        u, slot = t % HALF, t % SLOTS
+        first = unit_chunk(t % HALF)
+        window = pl.ds(pl.multiple_of(first * cols, 2 * cols), 2 * cols)
         return [
             pltpu.make_async_copy(
-                w_ref.at[:, span(ch, cols), :],
-                wbuf.at[slot, g, :, pl.ds(k * cols, cols), :], w_sem.at[slot, g, k])
-            for k, ch in enumerate((direct(u), swapped(u)))
+                w_ref.at[:, window, :], wbuf.at[t % SLOTS, g], w_sem.at[t % SLOTS, g])
             for g, w_ref in enumerate((wg_ref, wu_ref))
         ]
 
@@ -147,13 +159,13 @@
         blk = tok.at[swapped(j), across, band_rows(h)]
         return remote(blk, blk, z_send.at[h, j], z_recv.at[h, j], ep, zpeer)
 
-    def own_copy(h, ch):
-        blk = tok.at[ch, ep, band_rows(h)]
-        return remote(blk, blk, own_send.at[h, ch], own_recv.at[h, ch], partner, z)
-
-    def own_arrive(h, ch):
-        blk = tok.at[ch, partner, band_rows(h)]
-        return remote(blk, blk, own_send.at[h, ch], own_recv.at[h, ch], partner, z)
+    def own_copy(h, n):
+        blk = tok.at[pl.ds(n * HALF, HALF), ep, band_rows(h)]
+        return remote(blk, blk, own_send.at[h, n], own_recv.at[h, n], partner, z)
+
+    def own_arrive(h, n):
+        blk = tok.at[pl.ds(n * HALF, HALF), partner, band_rows(h)]
+        return remote(blk, blk, own_send.at[h, n], own_recv.at[h, n], partner, z)
 
     def fwd_copy(h, ch):
         blk = tok.at[ch, across, band_rows(h)]
@@ -175,9 +187,6 @@
         load_tok(direct(j)).start()
     for j in range(HALF):
         load_tok(swapped(j)).start()
-    for t in range(SLOTS):
-        for cp in load_unit(t):
-            cp.start()
 
     barrier = pltpu.get_barrier_semaphore()
     for e in peers:
@@ -201,28 +210,28 @@
     for e in range(4):
         meta[e, 0:experts, :] = slot[e * experts:(e + 1) * experts, :]
         meta[e, experts:2 * experts, :] = weight[e * experts:(e + 1) * experts, :]
+    for ch in range(CHUNKS):
+        load_tok(ch).wait()
+    for t in range(SLOTS):
+        for cp in load_unit(t):
+            cp.start()
+    for i in range(PIECES):
+        load_wd(i).start()
     pl.semaphore_wait(barrier, 6)
     for k, e in enumerate(peers):
         meta_copy(e, k).start()
-
-    for j in range(HALF):
-        load_tok(direct(j)).wait()
-        y_copy(0, j).start()
-        own_copy(0, direct(j)).start()
-    for j in range(HALF):
-        load_tok(swapped(j)).wait()
-        own_copy(0, swapped(j)).start()
-    for j in range(HALF):
-        y_copy(1, j).start()
-    for ch in range(CHUNKS):
-        own_copy(1, ch).start()
-    for i in range(PIECES):
-        load_wd(i).start()
+    for h in range(PASSES):
+        for j in range(HALF):
+            y_copy(h, j).start()
+        for n in range(2):
+            own_copy(h, n).start()
 
     meta_in[ep] = meta[ep]
     acc[...] = jnp.zeros_like(acc)
     for k, e in enumerate(peers):
         meta_arrive(e, k).wait_recv()
+    for n in range(2):
+        own_arrive(0, n).wait_recv()
 
     row_f = tri_r.astype(F32)
     for s in range(4):
@@ -244,9 +253,12 @@
 
     def unit(h, u):
         t = h * HALF + u
-        for k, ch in enumerate((direct(u), swapped(u))):
-            own_arrive(h, ch).wait_recv()
+        chunks = [unit_chunk(u) + k for k in range(2)]
+        for ch in chunks:
             fwd_arrive(h, ch).wait_recv()
+        for cp in load_unit(t):
+            cp.wait()
+        for k, ch in enumerate(chunks):
             for s in range(4):
                 x = jnp.dot(
                     place[h, s], tok[ch, s, band_rows(h), :],
@@ -254,31 +266,28 @@
                 for e in range(experts):
                     xr[e, s * CAP:(s + 1) * CAP, k * cols:(k + 1) * cols] = (
                         x[e * CAP:(e + 1) * CAP, :])
-        for cp in load_unit(t):
-            cp.wait()
-
-        def one(e, carry):
+        for e in range(experts):
             for g in range(2):
                 acc[g, e] += jnp.dot(xr[e], wbuf[t % SLOTS, g, e], preferred_element_type=F32)
-            return carry
-        lax.fori_loop(0, experts, one, 0)
 
         @pl.when(t + SLOTS < PASSES * HALF)
         def _():
             for cp in load_unit(t + SLOTS):
                 cp.start()
 
-    def relay(h, j):
-        @pl.when(j < HALF)
-        def _():
+    def relay(r):
+        @pl.when(r < PASSES * HALF)
+        def _():
+            h, j = r // HALF, r % HALF
             y_arrive(h, j).wait_recv()
             z_copy(h, j).start()
             fwd_copy(h, direct(j)).start()
 
-        @pl.when((j >= 1) & (j <= HALF))
-        def _():
-            z_arrive(h, j - 1).wait_recv()
-            fwd_copy(h, swapped(j - 1)).start()
+        @pl.when((r >= HOP) & (r < PASSES * HALF + HOP))
+        def _():
+            h, j = (r - HOP) // HALF, (r - HOP) % HALF
+            z_arrive(h, j).wait_recv()
+            fwd_copy(h, swapped(j)).start()
 
     def activate(h):
         def one(e, carry):
@@ -304,24 +313,19 @@
     def scatter_copy(h, i):
         return remote(
             part.at[i, c, y, band_rows(h)], z_in.at[i, band_rows(h)],
-            pz_send.at[h, i], pz_recv.at[h, i], ep, zshift(i))
+            pz_send.at[h, i], pz_recv.at[h, i], ep, next_hop(i))
 
     def down(h, i):
         if h == 0:
             load_wd(i).wait()
 
-        def one(e, carry):
+        for e in range(experts):
             o = jnp.dot(hid[e], wd[i, e], preferred_element_type=F32).astype(BF16)
             for s in range(4):
-                dnb[s, span(e, CAP), :] = o[s * CAP:(s + 1) * CAP, :]
-            return carry
-        lax.fori_loop(0, experts, one, 0)
-
-        def gather(s, carry):
+                dnb[s, e * CAP:(e + 1) * CAP, :] = o[s * CAP:(s + 1) * CAP, :]
+        for s in range(4):
             part[i, s % 2, s // 2, band_rows(h), :] = jnp.dot(
                 collect[h, s], dnb[s], preferred_element_type=F32).astype(BF16)
-            return carry
-        lax.fori_loop(0, 4, gather, 0)
         core_copy(h, i).start()
 
     def give_back(h, i):
@@ -334,42 +338,47 @@
         part[k, c, y, band_rows(h), :] += (
             core_in[k, y, band_rows(h), :] + y_in[k, band_rows(h), :])
 
+        @pl.when(k // 2 == 1)
+        def _():
+            scatter_copy(h, k - 2).wait_recv()
+            part[k, c, y, band_rows(h), :] += z_in[k - 2, band_rows(h), :]
+
         @pl.when(k < SENT)
         def _():
             scatter_copy(h, k).start()
 
-    def first_pass(j, carry):
-        relay(0, j)
-
-        @pl.when(j >= 2)
-        def _():
-            unit(0, j - 2)
+    for r in range(HOP):
+        relay(r)
+
+    def first_pass(u, carry):
+        @pl.when((u >= 1) & (u <= 2))
+        def _():
+            relay(2 * u)
+            relay(2 * u + 1)
+
+        @pl.when(u >= 3)
+        def _():
+            relay(u + HOP + 1)
+        unit(0, u)
         return carry
-    lax.fori_loop(0, HALF + 2, first_pass, 0)
+    lax.fori_loop(0, HALF, first_pass, 0)
     activate(0)
+    for n in range(2):
+        own_arrive(1, n).wait_recv()
 
     def second_pass(j, carry):
-        relay(1, j)
-
-        @pl.when((j >= 1) & (j <= PIECES))
-        def _():
-            give_back(0, j - 1)
-
-        @pl.when(j < PIECES)
-        def _():
-            down(0, j)
-
-        @pl.when(j >= 2)
-        def _():
-            unit(1, j - 2)
+        down(0, j)
+        for n in range(2):
+            relay(HALF + HOP + 1 + 2 * j + n)
+        unit(1, j)
+        give_back(0, j)
 
         @pl.when(j >= EARLY)
         def _():
             settle(0, j - EARLY)
         return carry
-    lax.fori_loop(0, HALF + 2, second_pass, 0)
+    lax.fori_loop(0, HALF, second_pass, 0)
     activate(1)
-    settled = HALF + 2 - EARLY
 
     def last_down(i, carry):
         @pl.when(i < PIECES)
@@ -380,9 +389,9 @@
         def _():
             give_back(1, i - 1)
 
-        @pl.when(i < PIECES - settled)
-        def _():
-            settle(0, i + settled)
+        @pl.when((i % 2 == 1) & (i >= 3) & (i < 3 + 2 * EARLY))
+        def _():
+            settle(0, PIECES - EARLY + (i - 3) // 2)
         return carry
     lax.fori_loop(0, PIECES + 1, last_down, 0)
 
@@ -394,7 +403,7 @@
     halves = []
     for n in range(2):
         half = part[SENT + n, c, y].astype(F32)
-        for i in range(n, SENT, 2):
+        for i in range(2 + n, SENT, 2):
             for h in range(PASSES):
                 scatter_copy(h, i).wait_recv()
             half += z_in[i].astype(F32)
@@ -433,10 +442,12 @@
             y_copy(h, j).wait_send()
             z_copy(h, j).wait_send()
             for ch in (direct(j), swapped(j)):
-                own_copy(h, ch).wait_send()
                 fwd_copy(h, ch).wait_send()
         return carry
     lax.fori_loop(0, HALF, sent_tokens, 0)
+    for h in range(PASSES):
+        for n in range(2):
+            own_copy(h, n).wait_send()
     for k, e in enumerate(peers):
         meta_copy(e, k).wait_send()
     for h in range(PASSES):
@@ -485,9 +496,8 @@
             pltpu.VMEM((3, 16, rows), F32),
             dma((CHUNKS,)), dma((PASSES, HALF)), dma((PASSES, HALF)),
             dma((PASSES, HALF)), dma((PASSES, HALF)),
-            dma((PASSES, CHUNKS)), dma((PASSES, CHUNKS)),
-            dma((PASSES, CHUNKS)), dma((PASSES, CHUNKS)),
-            dma((3,)), dma((3,)), dma((SLOTS, 2, 2)), dma((PIECES,)),
+            dma((PASSES, 2)), dma((PASSES, 2)), dma((PASSES, CHUNKS)), dma((PASSES, CHUNKS)),
+            dma((3,)), dma((3,)), dma((SLOTS, 2)), dma((PIECES,)),
             dma((PASSES, PIECES)), dma((PASSES, PIECES)),
             dma((PASSES, PIECES)), dma((PASSES, PIECES)),
             dma((PASSES, SENT)), dma((PASSES, SENT)), dma((3,)), dma((3,)),

time: 131 us -> 93.3 us (0.71)
  Pallas kernels: 129 us -> 91.2 us
    pallas_call x1, Pallas kernels: 129 us -> 91.2 us  [fused_on_device(): pl.pallas_call(moe_kernel, out_shape=jax.ShapeDtypeStruct((rows, piece),...]
where the time goes in v2:
time: 93.3 us; the launch traced here: 93.1 us
  Pallas kernels  91.2 us (98%)
  local copies, waits for them, and re-layouts  1.87 us (2%)
    pallas_call x1, Pallas kernels, fused_on_device(): pl.pallas_call(moe_kernel, out_shape=jax.ShapeDtypeStruct((rows, piece),...  91.2 us
    unnamed x1, local copies, waits for them, and re-layouts  1.87 us

profile of v2, /device:TPU:0, one launch (start us, length us, event | category | flops | bytes accessed | tf_op | source)
XLA Modules:
  0.0 93.1 jit_solution(2150397318763950337)
XLA Ops:
  0.0 91.2 %shard_map.82 = bf16[256,1024]{1,0:T(8,128)(2,1)} custom-call(s32[2,256]{1,0:T(2,128)} %bitcast.6, f32[2,256]{1,0:T(2,128)} %bitcast.7, f32[1,1024]{1,0:T(1,128)} %bitcast.4, f32[1,1024]{1,0:T(1,128)} %bitcast.5, bf16[256,4096]{1,0:T(8,128)(2,1)} %tokens_ref.1, bf16[4,4096,512]{2,1,0:T(8,128)(2,1)} %wg_ref.1, bf16[4,4096,512]{2,1,0:T(8,128)(2,1)} %wu_ref.1, ...), custom_call_target="tpu_custom_call" | custom-call | tf_op jit(solution)/shard_map/pallas_call | solution.py:473
  91.2 1.9 %copy.10 = bf16[256,1024]{1,0:T(8,128)(2,1)} copy(bf16[256,1024]{1,0:T(8,128)(2,1)} %shard_map.82) | data formatting | bytes 1048576

commit v3 on v2

--- a/solution.py
+++ b/solution.py
@@ -62,8 +62,20 @@
 SLOTS = 3
 PIECES = 8
 SENT = 6
-HOP = 2
-EARLY = 2
+FIRST_RELAYS = (
+    ((0, 1), ()), ((2, 3), (0, 1)), ((4, 5), ()), ((6,), (2, 3)),
+    ((7,), ()), ((8,), (4, 5)), ((9,), (6, 7)), ((10, 11, 12), (8,)),
+)
+SECOND_RELAYS = (
+    ((13, 14, 15), (9, 10)), ((), (11,)), ((), (12, 13)), ((), (14, 15)),
+    ((), ()), ((), ()), ((), ()), ((), ()),
+)
+SECOND_PIECES = (
+    ((0, 1), (), ()), ((2,), (), ()), ((3,), (0,), (0,)), ((4,), (1,), (1,)),
+    ((5,), (2,), ()), ((6,), (3,), (2,)), ((7,), (4,), (3,)), ((), (), (4,)),
+)
+LATE_SETTLES = ((4, 6), (6, 7))
+LAST = 6
 F32 = jnp.float32
 BF16 = jnp.bfloat16
 MESH = pl.DeviceIdType.MESH
@@ -73,10 +85,10 @@
     ids_ref, gates_ref, gain_ref, bias_ref, tokens_ref, wg_ref, wu_ref, wd_ref,
     out_ref,
     tok, wbuf, wd, acc, hid, xr, dnb, place, collect, rowg, meta, meta_in,
-    part, core_in, y_in, z_in, st_out, st_in,
+    part, core_in, y_in, z_in, pair_in, st_out, st_in,
     tok_sem, y_send, y_recv, z_send, z_recv, own_send, own_recv, fwd_send, fwd_recv,
     meta_send, meta_recv, w_sem, wd_sem, pc_send, pc_recv, py_send, py_recv,
-    pz_send, pz_recv, st_send, st_recv,
+    pz_send, pz_recv, pair_send, pair_recv, st_send, st_recv,
 ):
     ep = lax.axis_index("ep")
     z = lax.axis_index("tp")
@@ -109,14 +121,19 @@
     def band_rows(h):
         return pl.ds(pl.multiple_of(h * band, band), band)
 
+    inner = par + side - 2 * par * side
+    paired = 5 - 4 * inner
+    own = PIECES - 1
+
     def flip(far, near):
         return 2 * (side + far - 2 * side * far) + par + near - 2 * par * near
 
     def target(i):
-        return flip((3 - i // 2) // 2, (3 - i // 2) % 2)
-
-    def next_hop(i):
-        return flip((i // 2) % 2, 1 - (i // 2) % 2)
+        mask = (1 - inner) * (3 - i // 2) + inner * ((i // 2 + 1) % 4)
+        return flip(mask // 2, mask % 2)
+
+    def ranked(r):
+        return r + (1 - inner) * (r // 5) + inner * ((r + 6) // 7)
 
     def load_wd(i):
         return pltpu.make_async_copy(
@@ -270,24 +287,26 @@
             for g in range(2):
                 acc[g, e] += jnp.dot(xr[e], wbuf[t % SLOTS, g, e], preferred_element_type=F32)
 
-        @pl.when(t + SLOTS < PASSES * HALF)
-        def _():
+        if t + SLOTS < PASSES * HALF:
             for cp in load_unit(t + SLOTS):
                 cp.start()
 
-    def relay(r):
-        @pl.when(r < PASSES * HALF)
-        def _():
-            h, j = r // HALF, r % HALF
-            y_arrive(h, j).wait_recv()
-            z_copy(h, j).start()
-            fwd_copy(h, direct(j)).start()
-
-        @pl.when((r >= HOP) & (r < PASSES * HALF + HOP))
-        def _():
-            h, j = (r - HOP) // HALF, (r - HOP) % HALF
-            z_arrive(h, j).wait_recv()
-            fwd_copy(h, swapped(j)).start()
+    def relay_y(r):
+        h, j = r // HALF, r % HALF
+        y_arrive(h, j).wait_recv()
+        z_copy(h, j).start()
+        fwd_copy(h, direct(j)).start()
+
+    def relay_z(r):
+        h, j = r // HALF, r % HALF
+        z_arrive(h, j).wait_recv()
+        fwd_copy(h, swapped(j)).start()
+
+    def relay(ys, zs):
+        for r in ys:
+            relay_y(r)
+        for r in zs:
+            relay_z(r)
 
     def activate(h):
         def one(e, carry):
@@ -310,10 +329,18 @@
             part.at[i, c, 1 - y, band_rows(h)], y_in.at[i, band_rows(h)],
             py_send.at[h, i], py_recv.at[h, i], across, z)
 
+    def scatter_slot(h, slot, i, dest):
+        return remote(
+            part.at[i, c, y, band_rows(h)], z_in.at[slot, band_rows(h)],
+            pz_send.at[h, slot], pz_recv.at[h, slot], ep, dest)
+
     def scatter_copy(h, i):
-        return remote(
-            part.at[i, c, y, band_rows(h)], z_in.at[i, band_rows(h)],
-            pz_send.at[h, i], pz_recv.at[h, i], ep, next_hop(i))
+        onward = inner * ((i + 6) // 8)
+        return scatter_slot(
+            h, i + 2 * inner * (i // 4), i, zpeer + onward * (target(i) - zpeer))
+
+    def scattered(h, slot):
+        return scatter_slot(h, slot, 0, zpeer)
 
     def down(h, i):
         if h == 0:
@@ -328,114 +355,158 @@
                 collect[h, s], dnb[s], preferred_element_type=F32).astype(BF16)
         core_copy(h, i).start()
 
+    def pair_copy(n):
+        return remote(
+            part.at[paired, c, (1 - y) + n * (2 * y - 1), band_rows(1)], pair_in.at[n],
+            pair_send.at[n], pair_recv.at[n], ep, zpeer)
+
+    def give_pair():
+        core_copy(1, paired).wait_recv()
+        part[paired, c, :, band_rows(1), :] += core_in[paired, :, band_rows(1), :]
+        for n in range(2):
+            pair_copy(n).start()
+
+    def give_own():
+        core_copy(1, own).wait_recv()
+        pair_copy(0).wait_recv()
+        part[own, c, 1 - y, band_rows(1), :] += (
+            core_in[own, 1 - y, band_rows(1), :] + pair_in[0])
+        ret_copy(1, own).start()
+
     def give_back(h, i):
         core_copy(h, i).wait_recv()
         part[i, c, 1 - y, band_rows(h), :] += core_in[i, 1 - y, band_rows(h), :]
         ret_copy(h, i).start()
 
-    def settle(h, k):
-        ret_copy(h, k).wait_recv()
-        part[k, c, y, band_rows(h), :] += (
-            core_in[k, y, band_rows(h), :] + y_in[k, band_rows(h), :])
-
-        @pl.when(k // 2 == 1)
+    def settle(h, i):
+        ret_copy(h, i).wait_recv()
+        part[i, c, y, band_rows(h), :] += (
+            core_in[i, y, band_rows(h), :] + y_in[i, band_rows(h), :])
+
+        @pl.when((inner == 1) & (i >= 2) & (i < SENT))
         def _():
-            scatter_copy(h, k - 2).wait_recv()
-            part[k, c, y, band_rows(h), :] += z_in[k - 2, band_rows(h), :]
-
-        @pl.when(k < SENT)
+            scattered(h, i - 2).wait_recv()
+            part[i, c, y, band_rows(h), :] += z_in[i - 2, band_rows(h), :]
+
+        @pl.when(i < SENT)
         def _():
-            scatter_copy(h, k).start()
-
-    for r in range(HOP):
-        relay(r)
-
-    def first_pass(u, carry):
-        @pl.when((u >= 1) & (u <= 2))
-        def _():
-            relay(2 * u)
-            relay(2 * u + 1)
-
-        @pl.when(u >= 3)
-        def _():
-            relay(u + HOP + 1)
+            scatter_copy(h, i).start()
+
+    for u in range(HALF):
+        relay(*FIRST_RELAYS[u])
         unit(0, u)
-        return carry
-    lax.fori_loop(0, HALF, first_pass, 0)
     activate(0)
     for n in range(2):
         own_arrive(1, n).wait_recv()
 
-    def second_pass(j, carry):
-        down(0, j)
+    for u in range(HALF):
+        downs, outer_settles, inner_settles = SECOND_PIECES[u]
+        for i in downs:
+            down(0, i)
+        if u == 0:
+            give_back(0, 0)
+        relay(*SECOND_RELAYS[u])
+        unit(1, u)
+        for i in downs:
+            if i != 0:
+                give_back(0, i)
+        for v, settles in enumerate((outer_settles, inner_settles)):
+            for i in settles:
+                @pl.when(inner == v)
+                def _():
+                    settle(0, i)
+    activate(1)
+    settle(0, SENT - 1)
+
+    def nth(n):
+        second = (8 - n) // 7 - (7 - n) // 7
+        r = n - (n + 6) // 8
+        return second * paired + (1 - second) * ranked(r)
+
+    def last_down(n, carry):
+        @pl.when(n < PIECES)
+        def _():
+            down(1, nth(n))
+
+        @pl.when(n == 2)
+        def _():
+            give_pair()
+
+        @pl.when((n >= 1) & (n != 2))
+        def _():
+            give_back(1, nth(n - 1))
+        for step, i in LATE_SETTLES:
+            @pl.when(n == step)
+            def _():
+                settle(0, i)
+
+        @pl.when(n == 6 + inner)
+        def _():
+            settle(1, ranked(0))
+        return carry
+    lax.fori_loop(0, PIECES, last_down, 0)
+
+    def stat_copy(h, d):
+        return remote(
+            st_out.at[h], st_in.at[h, d - 1],
+            st_send.at[h, d - 1], st_recv.at[h, d - 1], ep, (z + d) % 4)
+
+    def collect_total(h):
         for n in range(2):
-            relay(HALF + HOP + 1 + 2 * j + n)
-        unit(1, j)
-        give_back(0, j)
-
-        @pl.when(j >= EARLY)
-        def _():
-            settle(0, j - EARLY)
+            half = part[SENT + n, c, y, band_rows(h), :].astype(F32)
+            for k in (n, 2 + n) if h == 0 or n == 0 else (2 + n,):
+                slot = 4 * inner + k
+                scattered(h, slot).wait_recv()
+                half += z_in[slot, band_rows(h), :].astype(F32)
+            acc[0, n, h * band:(h + 1) * band, :] = half
+
+    def send_stats(h):
+        mine = slice(h * band, (h + 1) * band)
+        total = jnp.concatenate([acc[0, n, mine, :] for n in range(2)], axis=1)
+        local_mean = jnp.sum(total, axis=1, keepdims=True) * (1.0 / piece)
+        gap = total - local_mean
+        local_m2 = jnp.sum(gap * gap, axis=1, keepdims=True)
+        st_out[h, 0:8, :] = jnp.broadcast_to(local_mean, (band, 128)).T[0:8, :]
+        st_out[h, 8:16, :] = jnp.broadcast_to(local_m2, (band, 128)).T[0:8, :]
+        for d in (1, 2, 3):
+            stat_copy(h, d).start()
+
+    def normalize(h):
+        mine = slice(h * band, (h + 1) * band)
+        for d in (1, 2, 3):
+            stat_copy(h, d).wait_recv()
+        means = [st_out[h, 0:8, :]] + [st_in[h, d, 0:8, :] for d in range(3)]
+        m2s = [st_out[h, 8:16, :]] + [st_in[h, d, 8:16, :] for d in range(3)]
+        mean = (means[0] + means[1] + means[2] + means[3]) * 0.25
+        m2 = m2s[0] + m2s[1] + m2s[2] + m2s[3]
+        for m in means:
+            m2 += (m - mean) * (m - mean) * piece
+        scale = lax.rsqrt(m2 * (1.0 / width) + norm_eps)
+        mean_col = jnp.broadcast_to(mean[0:1, :], (128, band)).T[:, 0:1]
+        scale_col = jnp.broadcast_to(scale[0:1, :], (128, band)).T[:, 0:1]
+        for n in range(2):
+            cut = slice(n * part_cols, (n + 1) * part_cols)
+            out_ref[mine, cut] = (
+                (acc[0, n, mine, :] - mean_col) * scale_col * gain_ref[:, cut]
+                + bias_ref[:, cut]).astype(BF16)
+
+    def last_settle(r, carry):
+        settle(1, ranked(r))
         return carry
-    lax.fori_loop(0, HALF, second_pass, 0)
-    activate(1)
-
-    def last_down(i, carry):
-        @pl.when(i < PIECES)
-        def _():
-            down(1, i)
-
-        @pl.when(i >= 1)
-        def _():
-            give_back(1, i - 1)
-
-        @pl.when((i % 2 == 1) & (i >= 3) & (i < 3 + 2 * EARLY))
-        def _():
-            settle(0, PIECES - EARLY + (i - 3) // 2)
-        return carry
-    lax.fori_loop(0, PIECES + 1, last_down, 0)
-
-    def last_settle(k, carry):
-        settle(1, k)
-        return carry
-    lax.fori_loop(0, PIECES, last_settle, 0)
-
-    halves = []
-    for n in range(2):
-        half = part[SENT + n, c, y].astype(F32)
-        for i in range(2 + n, SENT, 2):
-            for h in range(PASSES):
-                scatter_copy(h, i).wait_recv()
-            half += z_in[i].astype(F32)
-        halves.append(half)
-    total = jnp.concatenate(halves, axis=1)
-
-    local_mean = jnp.sum(total, axis=1, keepdims=True) * (1.0 / piece)
-    gap = total - local_mean
-    local_m2 = jnp.sum(gap * gap, axis=1, keepdims=True)
-    mean_t = jnp.broadcast_to(local_mean, (rows, 128)).T
-    m2_t = jnp.broadcast_to(local_m2, (rows, 128)).T
-    st_out[0:8, :] = mean_t[0:8, :]
-    st_out[8:16, :] = m2_t[0:8, :]
-
-    def stat_copy(d):
-        return remote(
-            st_out, st_in.at[d - 1], st_send.at[d - 1], st_recv.at[d - 1], ep, (z + d) % 4)
-    for d in (1, 2, 3):
-        stat_copy(d).start()
-    for d in (1, 2, 3):
-        stat_copy(d).wait_recv()
-    means = [st_out[0:8, :]] + [st_in[d, 0:8, :] for d in range(3)]
-    m2s = [st_out[8:16, :]] + [st_in[d, 8:16, :] for d in range(3)]
-    mean = (means[0] + means[1] + means[2] + means[3]) * 0.25
-    m2 = m2s[0] + m2s[1] + m2s[2] + m2s[3]
-    for m in means:
-        m2 += (m - mean) * (m - mean) * piece
-    scale = lax.rsqrt(m2 * (1.0 / width) + norm_eps)
-    mean_col = jnp.broadcast_to(mean[0:1, :], (128, rows)).T[:, 0:1]
-    scale_col = jnp.broadcast_to(scale[0:1, :], (128, rows)).T[:, 0:1]
-    out_ref[...] = (
-        (total - mean_col) * scale_col * gain_ref[...] + bias_ref[...]).astype(BF16)
+    lax.fori_loop(1, 2, last_settle, 0)
+    collect_total(0)
+    send_stats(0)
+    give_own()
+    lax.fori_loop(2, LAST - 1, last_settle, 0)
+    settle(1, ranked(LAST - 1))
+    ret_copy(1, own).wait_recv()
+    pair_copy(1).wait_recv()
+    part[own, c, y, band_rows(1), :] += (
+        core_in[own, y, band_rows(1), :] + y_in[own, band_rows(1), :] + pair_in[1])
+    collect_total(1)
+    send_stats(1)
+    normalize(0)
+    normalize(1)
 
     def sent_tokens(j, carry):
         for h in range(PASSES):
@@ -450,14 +521,21 @@
             own_copy(h, n).wait_send()
     for k, e in enumerate(peers):
         meta_copy(e, k).wait_send()
+    for n in range(2):
+        pair_copy(n).wait_send()
     for h in range(PASSES):
         for i in range(PIECES):
             core_copy(h, i).wait_send()
-            ret_copy(h, i).wait_send()
-        for i in range(SENT):
-            scatter_copy(h, i).wait_send()
-    for d in (1, 2, 3):
-        stat_copy(d).wait_send()
+        for d in (1, 2, 3):
+            stat_copy(h, d).wait_send()
+    for i in range(PIECES):
+        ret_copy(0, i).wait_send()
+        if i < SENT:
+            scatter_copy(0, i).wait_send()
+    for r in range(LAST + 1):
+        ret_copy(1, ranked(r)).wait_send()
+        if r < LAST - 1:
+            scatter_copy(1, ranked(r)).wait_send()
 
 
 def fused_on_device(tokens, expert_ids, gates, w_gate, w_up, w_down, norm_gain, norm_bias):
@@ -491,16 +569,18 @@
             pltpu.VMEM((PIECES, 2, 2, rows, part_cols), BF16),
             pltpu.VMEM((PIECES, 2, rows, part_cols), BF16),
             pltpu.VMEM((PIECES, rows, part_cols), BF16),
-            pltpu.VMEM((SENT, rows, part_cols), BF16),
-            pltpu.VMEM((16, rows), F32),
-            pltpu.VMEM((3, 16, rows), F32),
+            pltpu.VMEM((PIECES, rows, part_cols), BF16),
+            pltpu.VMEM((2, band, part_cols), BF16),
+            pltpu.VMEM((PASSES, 16, band), F32),
+            pltpu.VMEM((PASSES, 3, 16, band), F32),
             dma((CHUNKS,)), dma((PASSES, HALF)), dma((PASSES, HALF)),
             dma((PASSES, HALF)), dma((PASSES, HALF)),
             dma((PASSES, 2)), dma((PASSES, 2)), dma((PASSES, CHUNKS)), dma((PASSES, CHUNKS)),
             dma((3,)), dma((3,)), dma((SLOTS, 2)), dma((PIECES,)),
             dma((PASSES, PIECES)), dma((PASSES, PIECES)),
             dma((PASSES, PIECES)), dma((PASSES, PIECES)),
-            dma((PASSES, SENT)), dma((PASSES, SENT)), dma((3,)), dma((3,)),
+            dma((PASSES, PIECES)), dma((PASSES, PIECES)), dma((2,)), dma((2,)),
+            dma((PASSES, 3)), dma((PASSES, 3)),
         ],
         compiler_params=pltpu.CompilerParams(
             collective_id=0, has_side_effects=True, vmem_limit_bytes=64 * 1024 * 1024 - 65536),

time: 93.3 us -> 89.6 us (0.960)
  Pallas kernels: 91.2 us -> 87.5 us
    pallas_call x1, Pallas kernels: 91.2 us -> 87.5 us  [fused_on_device(): pl.pallas_call(moe_kernel, out_shape=jax.ShapeDtypeStruct((rows, piece),...]
where the time goes in v3:
time: 89.6 us; the launch traced here: 89.4 us
  Pallas kernels  87.5 us (98%)
  local copies, waits for them, and re-layouts  1.87 us (2%)
    pallas_call x1, Pallas kernels, fused_on_device(): pl.pallas_call(moe_kernel, out_shape=jax.ShapeDtypeStruct((rows, piece),...  87.5 us
    unnamed x1, local copies, waits for them, and re-layouts  1.87 us

profile of v3, /device:TPU:0, one launch (start us, length us, event | category | flops | bytes accessed | tf_op | source)
XLA Modules:
  0.0 89.4 jit_solution(12359102489022793311)
XLA Ops:
  0.0 87.5 %shard_map.82 = bf16[256,1024]{1,0:T(8,128)(2,1)} custom-call(s32[2,256]{1,0:T(2,128)} %bitcast.6, f32[2,256]{1,0:T(2,128)} %bitcast.7, f32[1,1024]{1,0:T(1,128)} %bitcast.4, f32[1,1024]{1,0:T(1,128)} %bitcast.5, bf16[256,4096]{1,0:T(8,128)(2,1)} %tokens_ref.1, bf16[4,4096,512]{2,1,0:T(8,128)(2,1)} %wg_ref.1, bf16[4,4096,512]{2,1,0:T(8,128)(2,1)} %wu_ref.1, ...), custom_call_target="tpu_custom_call" | custom-call | tf_op jit(solution)/shard_map/pallas_call | solution.py:551
  87.5 1.9 %copy.10 = bf16[256,1024]{1,0:T(8,128)(2,1)} copy(bf16[256,1024]{1,0:T(8,128)(2,1)} %shard_map.82) | data formatting | bytes 1048576

commit v4 on v3

--- a/solution.py
+++ b/solution.py
@@ -363,8 +363,11 @@
     def give_pair():
         core_copy(1, paired).wait_recv()
         part[paired, c, :, band_rows(1), :] += core_in[paired, :, band_rows(1), :]
-        for n in range(2):
-            pair_copy(n).start()
+        pair_copy(0).start()
+
+        @pl.when(inner == 1)
+        def _():
+            pair_copy(1).start()
 
     def give_own():
         core_copy(1, own).wait_recv()
@@ -416,7 +419,6 @@
                 def _():
                     settle(0, i)
     activate(1)
-    settle(0, SENT - 1)
 
     def nth(n):
         second = (8 - n) // 7 - (7 - n) // 7
@@ -439,6 +441,10 @@
             @pl.when(n == step)
             def _():
                 settle(0, i)
+
+        @pl.when(n == inner)
+        def _():
+            settle(0, SENT - 1)
 
         @pl.when(n == 6 + inner)
         def _():
@@ -498,6 +504,10 @@
     send_stats(0)
     give_own()
     lax.fori_loop(2, LAST - 1, last_settle, 0)
+
+    @pl.when(inner == 0)
+    def _():
+        pair_copy(1).start()
     settle(1, ranked(LAST - 1))
     ret_copy(1, own).wait_recv()
     pair_copy(1).wait_recv()
@@ -550,7 +560,7 @@
     hbm = pl.BlockSpec(memory_space=pl.ANY)
     return pl.pallas_call(
         moe_kernel,
-        out_shape=jax.ShapeDtypeStruct((rows, piece), jnp.bfloat16),
+        out_shape=pltpu.VMEM((rows, piece), jnp.bfloat16),
         in_specs=[vmem] * 4 + [hbm] * 4,
         out_specs=vmem,
         scratch_shapes=[
@@ -583,7 +593,7 @@
             dma((PASSES, 3)), dma((PASSES, 3)),
         ],
         compiler_params=pltpu.CompilerParams(
-            collective_id=0, has_side_effects=True, vmem_limit_bytes=64 * 1024 * 1024 - 65536),
+            collective_id=0, has_side_effects=True, vmem_limit_bytes=63 * 1024 * 1024),
     )(
         expert_ids.T, gates.T, norm_gain[None, :], norm_bias[None, :],
         tokens, w_gate, w_up, w_down,

time: 89.6 us -> 86.2 us (0.962)
  Pallas kernels: 87.5 us -> 85.2 us
  local copies, waits for them, and re-layouts: 1.87 us -> 0.8 us
    pallas_call x1, Pallas kernels: 87.5 us -> 85.2 us  [fused_on_device(): pl.pallas_call(moe_kernel, out_shape=pltpu.VMEM((rows, piece), jnp.bfloat...]
    unnamed x1, local copies, waits for them, and re-layouts: 1.87 us -> 0.8 us
where the time goes in v4:
time: 86.2 us; the launch traced here: 86 us
  Pallas kernels  85.2 us (99%)
    pallas_call x1, Pallas kernels, fused_on_device(): pl.pallas_call(moe_kernel, out_shape=pltpu.VMEM((rows, piece), jnp.bfloat...  85.2 us

profile of v4, /device:TPU:0, one launch (start us, length us, event | category | flops | bytes accessed | tf_op | source)
XLA Modules:
  0.0 86.0 jit_solution(14256729831859712374)
XLA Ops:
  0.0 85.2 %shard_map.82 = bf16[256,1024]{1,0:T(8,128)(2,1)S(1)} custom-call(s32[2,256]{1,0:T(2,128)} %bitcast.6, f32[2,256]{1,0:T(2,128)} %bitcast.7, f32[1,1024]{1,0:T(1,128)} %bitcast.4, f32[1,1024]{1,0:T(1,128)} %bitcast.5, bf16[256,4096]{1,0:T(8,128)(2,1)} %tokens_ref.1, bf16[4,4096,512]{2,1,0:T(8,128)(2,1)} %wg_ref.1, bf16[4,4096,512]{2,1,0:T(8,128)(2,1)} %wu_ref.1, ...), custom_call_target="tpu_custom_call" | custom-call | tf_op jit(solution)/shard_map/pallas_call | solution.py:561
  85.2 0.8 copy.10

commit v5 on v4

--- a/solution.py
+++ b/solution.py
@@ -244,7 +244,6 @@
             own_copy(h, n).start()
 
     meta_in[ep] = meta[ep]
-    acc[...] = jnp.zeros_like(acc)
     for k, e in enumerate(peers):
         meta_arrive(e, k).wait_recv()
     for n in range(2):
@@ -285,7 +284,8 @@
                         x[e * CAP:(e + 1) * CAP, :])
         for e in range(experts):
             for g in range(2):
-                acc[g, e] += jnp.dot(xr[e], wbuf[t % SLOTS, g, e], preferred_element_type=F32)
+                product = jnp.dot(xr[e], wbuf[t % SLOTS, g, e], preferred_element_type=F32)
+                acc[g, e] = product if u == 0 else acc[g, e] + product
 
         if t + SLOTS < PASSES * HALF:
             for cp in load_unit(t + SLOTS):
@@ -313,9 +313,6 @@
             g = acc[0, e]
             v = g / (1.0 + jnp.exp(-g)) * acc[1, e]
             hid[e] = (v * rowg[h, e][:, 0:1]).astype(BF16)
-            if h + 1 < PASSES:
-                acc[0, e] = jnp.zeros_like(g)
-                acc[1, e] = jnp.zeros_like(g)
             return carry
         lax.fori_loop(0, experts, one, 0)
 
@@ -503,11 +500,12 @@
     collect_total(0)
     send_stats(0)
     give_own()
-    lax.fori_loop(2, LAST - 1, last_settle, 0)
+    lax.fori_loop(2, LAST - 2, last_settle, 0)
 
     @pl.when(inner == 0)
     def _():
         pair_copy(1).start()
+    settle(1, ranked(LAST - 2))
     settle(1, ranked(LAST - 1))
     ret_copy(1, own).wait_recv()
     pair_copy(1).wait_recv()

time: 86.2 us -> 86 us (level)
  no operation moved by 1% of the time
where the time goes in v5:
time: 86 us; the launch traced here: 85.8 us
  Pallas kernels  85 us (99%)
    pallas_call x1, Pallas kernels, fused_on_device(): pl.pallas_call(moe_kernel, out_shape=pltpu.VMEM((rows, piece), jnp.bfloat...  85 us

profile of v5, /device:TPU:0, one launch (start us, length us, event | category | flops | bytes accessed | tf_op | source)
XLA Modules:
  0.0 85.8 jit_solution(16942320932447375517)
XLA Ops:
  0.0 85.0 %shard_map.82 = bf16[256,1024]{1,0:T(8,128)(2,1)S(1)} custom-call(s32[2,256]{1,0:T(2,128)} %bitcast.6, f32[2,256]{1,0:T(2,128)} %bitcast.7, f32[1,1024]{1,0:T(1,128)} %bitcast.4, f32[1,1024]{1,0:T(1,128)} %bitcast.5, bf16[256,4096]{1,0:T(8,128)(2,1)} %tokens_ref.1, bf16[4,4096,512]{2,1,0:T(8,128)(2,1)} %wg_ref.1, bf16[4,4096,512]{2,1,0:T(8,128)(2,1)} %wu_ref.1, ...), custom_call_target="tpu_custom_call" | custom-call | tf_op jit(solution)/shard_map/pallas_call | solution.py:559
  85.0 0.8 copy.10
